TPU v7x, 32 devices: a whole 2x2x4 slice. The times are simulated.
32 devices in a mesh: rep: 4 (over z), fs: 4 (over y, x), tp: 2 (over core).
Axes of the slice: x: 2, y: 2, z: 4, core: 2. Of those that a mesh axis runs over, the one named last changes fastest.
Arguments:
- tokens: bfloat16 [8192, 2048], P(('rep', 'fs')), may hold values from -6 to 6
- mix_gain: float32 [2048], replicated, may hold values from 0.1 to 1.9
- w_gate_b: bfloat16 [2048, 1024], P('fs', 'tp'), may hold values from -0.125 to 0.125
- w_gate_c: bfloat16 [2048, 1024], P('fs', 'tp'), may hold values from -0.125 to 0.125
- w_conv_in: bfloat16 [2048, 1024], P('fs', 'tp'), may hold values from -0.125 to 0.125
- conv_taps: float32 [3, 1024], P(None, 'tp'), may hold values from -3 to 3
- w_mix_out: bfloat16 [1024, 2048], P('tp', 'fs'), may hold values from -0.1875 to 0.1875
- ffn_gain: float32 [2048], replicated, may hold values from 0.1 to 1.9
- w_ffn_gate: bfloat16 [2048, 2816], P('fs', 'tp'), may hold values from -0.125 to 0.125
- w_ffn_up: bfloat16 [2048, 2816], P('fs', 'tp'), may hold values from -0.125 to 0.125
- w_ffn_down: bfloat16 [2816, 2048], P('tp', 'fs'), may hold values from -0.109375 to 0.109375
Outputs:
- layer_out: bfloat16 [8192, 2048], P(('rep', 'fs', 'tp'))
All inputs are finite; a program needn't handle non-finite values.
Results may differ from a plain program's by a relative error of at most 0.014.
Values may be sent and summed in bfloat16 or wider, within the bound.
A program may use at most 64 MiB of HBM per device.

v0:
```python
import jax
import jax.numpy as jnp
from jax import lax
from jax.sharding import PartitionSpec as P

LEN = 128
EPSILON = 1e-06


def rms_scale(values, gain):
    return values * lax.rsqrt(jnp.mean(values * values, axis=-1, keepdims=True) + EPSILON) * gain


def causal_mix(product_in, conv_taps):
    shaped = product_in.reshape(product_in.shape[0] // LEN, LEN, product_in.shape[1])
    padded = jnp.pad(shaped, ((0, 0), (2, 0), (0, 0)))
    convolved = (
        conv_taps[0] * padded[:, :-2]
        + conv_taps[1] * padded[:, 1:-1]
        + conv_taps[2] * padded[:, 2:]
    )
    return convolved.reshape(product_in.shape)


def local(
    tokens,
    mix_gain,
    w_gate_b,
    w_gate_c,
    w_conv_in,
    conv_taps,
    w_mix_out,
    ffn_gain,
    w_ffn_gate,
    w_ffn_up,
    w_ffn_down,
):
    normed = rms_scale(tokens.astype(jnp.float32), mix_gain).astype(jnp.bfloat16)
    shard_rows = (
        lax.all_gather(w_gate_b, "fs", axis=0, tiled=True),
        lax.all_gather(w_gate_c, "fs", axis=0, tiled=True),
        lax.all_gather(w_conv_in, "fs", axis=0, tiled=True),
    )
    gate_b, gate_c, conv_in = tuple(
        (jnp.dot(normed, weight, preferred_element_type=jnp.float32) for weight in shard_rows)
    )
    gated = (gate_b * causal_mix(gate_c * conv_in, conv_taps)).astype(jnp.bfloat16)
    mix_columns = lax.all_gather(w_mix_out, "fs", axis=1, tiled=True)
    row_count = normed.shape[0] // lax.axis_size("tp")
    branch = lax.psum_scatter(
        jnp.dot(gated, mix_columns, preferred_element_type=jnp.float32).astype(jnp.bfloat16),
        "tp",
        scatter_dimension=0,
        tiled=True,
    ).astype(jnp.float32)
    own_rows = lax.dynamic_slice_in_dim(tokens, lax.axis_index("tp") * row_count, row_count, 0)
    stream = own_rows.astype(jnp.float32) + branch
    normed_two = rms_scale(stream, ffn_gain).astype(jnp.bfloat16)
    gate_rows, up_rows = (
        lax.all_gather(w_ffn_gate, "fs", axis=0, tiled=True),
        lax.all_gather(w_ffn_up, "fs", axis=0, tiled=True),
    )
    shard_rows = lax.all_gather(normed_two, "tp", axis=0, tiled=True)
    gate_part = jnp.dot(shard_rows, gate_rows, preferred_element_type=jnp.float32)
    up_part = jnp.dot(shard_rows, up_rows, preferred_element_type=jnp.float32)
    hidden = (jax.nn.silu(gate_part) * up_part).astype(jnp.bfloat16)
    down_columns = lax.all_gather(w_ffn_down, "fs", axis=1, tiled=True)
    ffn_branch = lax.psum_scatter(
        jnp.dot(hidden, down_columns, preferred_element_type=jnp.float32).astype(jnp.bfloat16),
        "tp",
        scatter_dimension=0,
        tiled=True,
    ).astype(jnp.float32)
    return (stream + ffn_branch).astype(jnp.bfloat16)


def solution(mesh):
    in_specs = (
        P(("rep", "fs"), None),
        P(),
        P("fs", "tp"),
        P("fs", "tp"),
        P("fs", "tp"),
        P(None, "tp"),
        P("tp", "fs"),
        P(),
        P("fs", "tp"),
        P("fs", "tp"),
        P("tp", "fs"),
    )
    out_specs = P(("rep", "fs", "tp"), None)
    return jax.shard_map(local, mesh=mesh, in_specs=in_specs, out_specs=out_specs, check_vma=False)
```

profile of v0, /device:TPU:0, one launch (start us, length us, event | category | flops | bytes accessed | tf_op | source)
XLA Modules:
  0.0 424.1 jit_solution(1093069393383213584)
XLA Ops:
  6.5 0.7 all-gather.11.cloned.1.call-update
  7.3 0.7 all-gather.13.cloned.1.call-update
  8.1 0.7 all-gather.15.cloned.1.call-update
  9.9 37.2 %all-gather.11.cloned.1.call-done = bf16[2048,512]{1,0:T(8,128)(2,1)} async-done(((bf16[512,512]{1,0:T(8,128)(2,1)}), bf16[2048,512]{1,0:T(8,128)(2,1)}) %all-gather.11.cloned.1.call-update) | async-done | bytes 2097168 | tf_op jit(solution)/shard_map/all_gather | solution.py:41
  47.1 2.9 fusion.11
  50.0 34.2 %all-gather.13.cloned.1.call-done = bf16[2048,512]{1,0:T(8,128)(2,1)} async-done(((bf16[512,512]{1,0:T(8,128)(2,1)}), bf16[2048,512]{1,0:T(8,128)(2,1)}) %all-gather.13.cloned.1.call-update) | async-done | bytes 2097168 | tf_op jit(solution)/shard_map/all_gather | solution.py:42
  84.2 2.9 convolution_multiply_fusion.1
  87.4 33.7 %all-gather.15.cloned.1.call-done = bf16[512,2048]{1,0:T(8,128)(2,1)} async-done(((bf16[512,512]{1,0:T(8,128)(2,1)}), bf16[512,2048]{1,0:T(8,128)(2,1)}) %all-gather.15.cloned.1.call-update) | async-done | bytes 2097168 | tf_op jit(solution)/shard_map/all_gather | solution.py:48
  121.1 36.9 %all-gather.9.cloned.1.call-done = bf16[2048,512]{1,0:T(8,128)(2,1)} async-done(((bf16[512,512]{1,0:T(8,128)(2,1)}), bf16[2048,512]{1,0:T(8,128)(2,1)}) %all-gather.9.cloned.1.call-update) | async-done | bytes 2097168 | tf_op jit(solution)/shard_map/all_gather | solution.py:40
  158.0 5.9 %convolution_convert_fusion = bf16[512,2048]{1,0:T(8,128)(2,1)} fusion(bf16[512,2048]{1,0:T(8,128)(2,1)} %all-gather.15.cloned.1.call-done, f32[512,512]{1,0:T(8,128)S(1)} %bitcast.14, bf16[2048,512]{1,0:T(8,128)(2,1)} %all-gather.9.cloned.1.call-done, bf16[512,2048]{1,0:T(8,128)(2,1)S(1)} %copy-done, f32[2048]{0:T(1024)S(1)} %copy-done.4, ...), kind=kOutput, calls=%fused_computation.7 | convolution fusion | flops 2153250816 | bytes 9447424 | tf_op jit(solution)/shard_map/dot_general | solution.py:51
  164.0 0.5 all-gather.19.cloned.1.call-update
  164.6 9.3 %reduce-scatter.3.cloned.1.call-done = bf16[256,2048]{1,0:T(8,128)(2,1)} async-done(((bf16[512,2048]{1,0:T(8,128)(2,1)}), bf16[256,2048]{1,0:T(8,128)(2,1)}) %reduce-scatter.3.cloned.1.call-update) | async-done | bytes 1048592 | tf_op jit(solution)/shard_map/reduce_scatter | solution.py:50
  173.9 1.7 multiply_reduce_fusion
  175.6 1.5 multiply_convert_fusion
  177.2 0.7 all-gather.21.cloned.1.call-update
  177.9 0.7 all-gather.23.cloned.1.call-update
  178.8 63.7 %all-gather.19.cloned.1.call-done = bf16[2048,1408]{1,0:T(8,128)(2,1)} async-done(((bf16[512,1408]{1,0:T(8,128)(2,1)}), bf16[2048,1408]{1,0:T(8,128)(2,1)}) %all-gather.19.cloned.1.call-update) | async-done | bytes 5767184 | tf_op jit(solution)/shard_map/all_gather | solution.py:60
  242.5 12.1 %all-gather.17.cloned.1.call-done = bf16[512,2048]{1,0:T(8,128)(2,1)} async-done(((bf16[256,2048]{1,0:T(8,128)(2,1)}), bf16[512,2048]{1,0:T(8,128)(2,1)}) %all-gather.17.cloned.1.call-update) | async-done | bytes 2097168 | tf_op jit(solution)/shard_map/all_gather | solution.py:63
  254.7 8.2 %fusion.16 = f32[512,1408]{1,0:T(8,128)} fusion(bf16[512,2048]{1,0:T(8,128)(2,1)} %all-gather.17.cloned.1.call-done, bf16[2048,1408]{1,0:T(8,128)(2,1)} %all-gather.19.cloned.1.call-done), kind=kOutput, calls=%fused_computation.27 | convolution fusion | flops 2952790016 | bytes 10747904 | tf_op jit(solution)/shard_map/dot_general | solution.py:64
  262.9 60.5 %all-gather.21.cloned.1.call-done = bf16[2048,1408]{1,0:T(8,128)(2,1)} async-done(((bf16[512,1408]{1,0:T(8,128)(2,1)}), bf16[2048,1408]{1,0:T(8,128)(2,1)}) %all-gather.21.cloned.1.call-update) | async-done | bytes 5767184 | tf_op jit(solution)/shard_map/all_gather | solution.py:61
  323.4 67.4 %all-gather.23.cloned.1.call-done = bf16[1408,2048]{1,0:T(8,128)(2,1)} async-done(((bf16[1408,512]{1,0:T(8,128)(2,1)}), bf16[1408,2048]{1,0:T(8,128)(2,1)}) %all-gather.23.cloned.1.call-update) | async-done | bytes 5767184 | tf_op jit(solution)/shard_map/all_gather | solution.py:67
  390.8 13.8 %convolution_convert_fusion.1 = bf16[512,2048]{1,0:T(8,128)(2,1)} fusion(bf16[1408,2048]{1,0:T(8,128)(2,1)} %all-gather.23.cloned.1.call-done, bf16[512,2048]{1,0:T(8,128)(2,1)} %all-gather.17.cloned.1.call-done, bf16[2048,1408]{1,0:T(8,128)(2,1)} %all-gather.21.cloned.1.call-done, f32[512,1408]{1,0:T(8,128)} %fusion.16), kind=kOutput, calls=%fused_computation.8 | convolution fusion | flops 5910953984 | bytes 18612224 | tf_op jit(solution)/shard_map/dot_general | solution.py:69
  404.6 9.9 %reduce-scatter.5.cloned.1.call-done = bf16[256,2048]{1,0:T(8,128)(2,1)} async-done(((bf16[512,2048]{1,0:T(8,128)(2,1)}), bf16[256,2048]{1,0:T(8,128)(2,1)}) %reduce-scatter.5.cloned.1.call-update) | async-done | bytes 1048592 | tf_op jit(solution)/shard_map/reduce_scatter | solution.py:68
  414.5 2.7 add_convert_fusion
  (29 shorter events, 1.9 us)
Async XLA Ops:
  6.5 2.8 copy-start
  6.5 40.6 %all-gather.11.cloned.1.call-start = ((), (), s32[]{:S(2)}) async-start(), calls=%async_computation.3 | async-start | bytes 2621440 | tf_op jit(solution)/shard_map/all_gather | solution.py:41
  6.5 3.3 copy-start.3
  6.5 40.6 %copy-start.4 = (f32[2048]{0:T(1024)S(1)}, f32[2048]{0:T(1024)}, u32[]{:S(2)}) copy-start(f32[2048]{0:T(1024)} %param.12) | copy-start | bytes 24580
  7.3 76.9 %all-gather.13.cloned.1.call-start = ((), (), s32[]{:S(2)}) async-start(), calls=%async_computation.4 | async-start | bytes 2621440 | tf_op jit(solution)/shard_map/all_gather | solution.py:42
  8.0 113.1 %all-gather.15.cloned.1.call-start = ((), (), s32[]{:S(2)}) async-start(), calls=%async_computation.5 | async-start | bytes 2621440 | tf_op jit(solution)/shard_map/all_gather | solution.py:48
  8.7 149.2 %all-gather.9.cloned.1.call-start = ((), (), s32[]{:S(2)}) async-start(), calls=%async_computation.2 | async-start | bytes 2621440 | tf_op jit(solution)/shard_map/all_gather | solution.py:40
  9.3 164.5 %reduce-scatter.3.cloned.1.call-start = ((), (), s32[]{:S(2)}) async-start(), calls=%async_computation.6 | async-start | bytes 3145728 | tf_op jit(solution)/shard_map/reduce_scatter | solution.py:50
  163.9 11.7 %copy-start.2 = (f32[2048]{0:T(1024)S(1)}, f32[2048]{0:T(1024)}, u32[]{:S(2)}) copy-start(f32[2048]{0:T(1024)} %param.18) | copy-start | bytes 24580
  164.0 78.6 %all-gather.19.cloned.1.call-start = ((), (), s32[]{:S(2)}) async-start(), calls=%async_computation.8 | async-start | bytes 7208960 | tf_op jit(solution)/shard_map/all_gather | solution.py:60
  164.5 90.2 %all-gather.17.cloned.1.call-start = ((), (), s32[]{:S(2)}) async-start(), calls=%async_computation.7 | async-start | bytes 3145728 | tf_op jit(solution)/shard_map/all_gather | solution.py:63
  173.9 1.8 copy-start.1
  177.1 146.3 %all-gather.21.cloned.1.call-start = ((), (), s32[]{:S(2)}) async-start(), calls=%async_computation.9 | async-start | bytes 7208960 | tf_op jit(solution)/shard_map/all_gather | solution.py:61
  177.9 212.9 %all-gather.23.cloned.1.call-start = ((), (), s32[]{:S(2)}) async-start(), calls=%async_computation.10 | async-start | bytes 7208960 | tf_op jit(solution)/shard_map/all_gather | solution.py:67
  178.6 235.9 %reduce-scatter.5.cloned.1.call-start = ((), (), s32[]{:S(2)}) async-start(), calls=%async_computation.11 | async-start | bytes 3145728 | tf_op jit(solution)/shard_map/reduce_scatter | solution.py:68
Sparse Core Ops, SparseCore 0:
  9.2 37.8 all-gather.10
  49.0 35.1 all-gather.12
  86.0 35.0 all-gather.14
  122.8 35.1 all-gather.8
  164.1 9.7 reduce-scatter.2
  175.6 66.9 all-gather.18
  244.1 10.5 all-gather.16
  256.5 66.8 all-gather.20
  325.2 65.5 all-gather.22
  404.8 9.7 reduce-scatter.4
where the time goes:
time: 424 us
  waiting for transfers between devices  369 us (87%)
  matrix products  33.8 us (8%)
  between operations  13.6 us (3%)
  other arithmetic  6.75 us (2%)
    all_gather x1, waiting for transfers between devices, local(): down_columns = lax.all_gather(w_ffn_down, 'fs', axis=1, tiled=True)  67.4 us
    all_gather x1, waiting for transfers between devices, local(): lax.all_gather(w_ffn_gate, 'fs', axis=0, tiled=True)  63.7 us
    all_gather x1, waiting for transfers between devices, local(): lax.all_gather(w_ffn_up, 'fs', axis=0, tiled=True)  60.5 us
    all_gather x1, waiting for transfers between devices, local(): lax.all_gather(w_gate_c, 'fs', axis=0, tiled=True)  37.2 us
    all_gather x1, waiting for transfers between devices, local(): lax.all_gather(w_gate_b, 'fs', axis=0, tiled=True)  36.9 us
    all_gather x1, waiting for transfers between devices, local(): lax.all_gather(w_conv_in, 'fs', axis=0, tiled=True)  34.2 us
    all_gather x1, waiting for transfers between devices, local(): mix_columns = lax.all_gather(w_mix_out, 'fs', axis=1, tiled=True)  33.7 us
    dot_general x1, matrix products, local(): jnp.dot(hidden, down_columns, preferred_element_type=jnp.float32)  13.8 us
  transfers between devices with their start and end apart: 10, of which 10 were waited for; matrix products, arithmetic and copies ran while one was open for 4% of the time, Pallas kernels for 0%

commit v1 on v0

--- a/solution.py
+++ b/solution.py
@@ -64,7 +64,12 @@
     gate_part = jnp.dot(shard_rows, gate_rows, preferred_element_type=jnp.float32)
     up_part = jnp.dot(shard_rows, up_rows, preferred_element_type=jnp.float32)
     hidden = (jax.nn.silu(gate_part) * up_part).astype(jnp.bfloat16)
-    down_columns = lax.all_gather(w_ffn_down, "fs", axis=1, tiled=True)
+    ring = [w_ffn_down]
+    for hop in range(3):
+        ring.append(lax.ppermute(ring[-1], "fs", [(dev, (dev + 1) % 4) for dev in range(4)]))
+    down_columns = jnp.roll(
+        jnp.concatenate(ring[::-1], axis=1), (lax.axis_index("fs") + 1) * ring[0].shape[1], axis=1
+    )
     ffn_branch = lax.psum_scatter(
         jnp.dot(hidden, down_columns, preferred_element_type=jnp.float32).astype(jnp.bfloat16),
         "tp",

time: 424 us -> 412 us (0.972)
  waiting for transfers between devices: 369 us -> 335 us
  local copies, waits for them, and re-layouts: 0.03 us -> 17.6 us
  starting transfers between devices: 0.53 us -> 5.31 us
    ppermute x0 -> x3, waiting for transfers between devices: none -> 154 us  [local(): lax.ppermute(ring[-1], 'fs', [(dev, (dev + 1) % 4) for dev in range(4)])]
    all_gather x1 -> x0, waiting for transfers between devices: 67.4 us -> none  [local(): down_columns = lax.all_gather(w_ffn_down, 'fs', axis=1, tiled=True)]
    all_gather x1, waiting for transfers between devices: 63.7 us -> 0.01 us  [local(): lax.all_gather(w_ffn_gate, 'fs', axis=0, tiled=True)]
    all_gather x1, waiting for transfers between devices: 60.5 us -> 15.8 us  [local(): lax.all_gather(w_ffn_up, 'fs', axis=0, tiled=True)]
    unnamed x10 -> x23, local copies, waits for them, and re-layouts: 0.02 us -> 16.3 us
    all_gather x1, waiting for transfers between devices: 12.1 us -> 0.01 us  [local(): shard_rows = lax.all_gather(normed_two, 'tp', axis=0, tiled=True)]
    ppermute x0 -> x3, starting transfers between devices: none -> 4.99 us  [local(): lax.ppermute(ring[-1], 'fs', [(dev, (dev + 1) % 4) for dev in range(4)])]
  transfers between devices with their start and end apart: 10 -> 12, of which waited for: 10 -> 10; matrix products, arithmetic and copies ran while one was open for 4% -> 8% of each run, Pallas kernels for 0% -> 0%
where the time goes in v1:
time: 412 us
  waiting for transfers between devices  335 us (81%)
  matrix products  34.1 us (8%)
  local copies, waits for them, and re-layouts  17.6 us (4%)
  between operations  13.3 us (3%)
  other arithmetic  6.75 us (2%)
  starting transfers between devices  5.31 us (1%)
    ppermute x3, waiting for transfers between devices, local(): lax.ppermute(ring[-1], 'fs', [(dev, (dev + 1) % 4) for dev in range(4)])  154 us
    all_gather x1, waiting for transfers between devices, local(): lax.all_gather(w_gate_c, 'fs', axis=0, tiled=True)  37.2 us
    all_gather x1, waiting for transfers between devices, local(): lax.all_gather(w_gate_b, 'fs', axis=0, tiled=True)  36.9 us
    all_gather x1, waiting for transfers between devices, local(): lax.all_gather(w_conv_in, 'fs', axis=0, tiled=True)  34.2 us
    all_gather x1, waiting for transfers between devices, local(): mix_columns = lax.all_gather(w_mix_out, 'fs', axis=1, tiled=True)  33.7 us
    unnamed x23, local copies, waits for them, and re-layouts  16.3 us
    all_gather x1, waiting for transfers between devices, local(): lax.all_gather(w_ffn_up, 'fs', axis=0, tiled=True)  15.8 us
    dot_general x1, matrix products, local(): jnp.dot(hidden, down_columns, preferred_element_type=jnp.float32)  14 us
  transfers between devices with their start and end apart: 12, of which 10 were waited for; matrix products, arithmetic and copies ran while one was open for 8% of the time, Pallas kernels for 0%

profile of v1, /device:TPU:0, one launch (start us, length us, event | category | flops | bytes accessed | tf_op | source)
XLA Modules:
  0.0 411.6 jit_solution(6324177853650509527)
XLA Ops:
  9.9 37.2 %all-gather.10.cloned.1.call-done = bf16[2048,512]{1,0:T(8,128)(2,1)} async-done(((bf16[512,512]{1,0:T(8,128)(2,1)}), bf16[2048,512]{1,0:T(8,128)(2,1)}) %all-gather.10.cloned.1.call-update) | async-done | bytes 2097168 | tf_op jit(solution)/shard_map/all_gather | solution.py:41
  47.1 2.9 fusion.17
  50.0 34.2 %all-gather.12.cloned.1.call-done = bf16[2048,512]{1,0:T(8,128)(2,1)} async-done(((bf16[512,512]{1,0:T(8,128)(2,1)}), bf16[2048,512]{1,0:T(8,128)(2,1)}) %all-gather.12.cloned.1.call-update) | async-done | bytes 2097168 | tf_op jit(solution)/shard_map/all_gather | solution.py:42
  84.2 2.9 convolution_multiply_fusion.1
  87.4 33.7 %all-gather.14.cloned.1.call-done = bf16[512,2048]{1,0:T(8,128)(2,1)} async-done(((bf16[512,512]{1,0:T(8,128)(2,1)}), bf16[512,2048]{1,0:T(8,128)(2,1)}) %all-gather.14.cloned.1.call-update) | async-done | bytes 2097168 | tf_op jit(solution)/shard_map/all_gather | solution.py:48
  121.1 36.9 %all-gather.8.cloned.1.call-done = bf16[2048,512]{1,0:T(8,128)(2,1)} async-done(((bf16[512,512]{1,0:T(8,128)(2,1)}), bf16[2048,512]{1,0:T(8,128)(2,1)}) %all-gather.8.cloned.1.call-update) | async-done | bytes 2097168 | tf_op jit(solution)/shard_map/all_gather | solution.py:40
  158.0 6.0 %convolution_convert_fusion = bf16[512,2048]{1,0:T(8,128)(2,1)} fusion(bf16[512,2048]{1,0:T(8,128)(2,1)} %all-gather.14.cloned.1.call-done, f32[512,512]{1,0:T(8,128)S(1)} %bitcast.13, bf16[2048,512]{1,0:T(8,128)(2,1)} %all-gather.8.cloned.1.call-done, bf16[512,2048]{1,0:T(8,128)(2,1)S(1)} %copy-done, f32[2048]{0:T(1024)S(1)} %copy-done.7, ...), kind=kOutput, calls=%fused_computation.10 | convolution fusion | flops 2153250816 | bytes 9447424 | tf_op jit(solution)/shard_map/dot_general | solution.py:51
  164.6 9.2 %reduce-scatter.3.cloned.1.call-done = bf16[256,2048]{1,0:T(8,128)(2,1)} async-done(((bf16[512,2048]{1,0:T(8,128)(2,1)}), bf16[256,2048]{1,0:T(8,128)(2,1)}) %reduce-scatter.3.cloned.1.call-update) | async-done | bytes 1048592 | tf_op jit(solution)/shard_map/reduce_scatter | solution.py:50
  173.9 1.7 multiply_reduce_fusion
  175.6 1.5 multiply_convert_fusion
  177.9 1.9 collective-permute-start
  179.8 50.1 %collective-permute-done = bf16[1408,512]{1,0:T(8,128)(2,1)S(1)} collective-permute-done((bf16[1408,512]{1,0:T(8,128)(2,1)}, bf16[1408,512]{1,0:T(8,128)(2,1)S(1)}, u32[]{:S(2)}, u32[]{:S(2)}) %collective-permute-start) | collective-permute-done | bytes 1441824 | tf_op jit(solution)/shard_map/ppermute | solution.py:69
  231.1 2.3 collective-permute-start.1
  233.5 56.8 %collective-permute-done.1 = bf16[1408,512]{1,0:T(8,128)(2,1)} collective-permute-done((bf16[1408,512]{1,0:T(8,128)(2,1)S(1)}, bf16[1408,512]{1,0:T(8,128)(2,1)}, u32[]{:S(2)}, u32[]{:S(2)}) %collective-permute-start.1) | collective-permute-done | bytes 1441824 | tf_op jit(solution)/shard_map/ppermute | solution.py:69
  291.0 46.8 %collective-permute-done.2 = bf16[1408,512]{1,0:T(8,128)(2,1)} collective-permute-done((bf16[1408,512]{1,0:T(8,128)(2,1)}, bf16[1408,512]{1,0:T(8,128)(2,1)}, u32[]{:S(2)}, u32[]{:S(2)}) %collective-permute-start.2) | collective-permute-done | bytes 1441824 | tf_op jit(solution)/shard_map/ppermute | solution.py:69
  337.8 2.7 constant_dynamic-update-slice_fusion.7
  340.5 2.8 constant_dynamic-update-slice_fusion.6
  346.4 2.7 constant_dynamic-update-slice_fusion.3
  349.0 2.6 constant_dynamic-update-slice_fusion.2
  354.3 8.3 %fusion.22 = f32[512,1408]{1,0:T(8,128)} fusion(bf16[512,2048]{1,0:T(8,128)(2,1)} %all-gather.16.cloned.1.call-done, bf16[2048,1408]{1,0:T(8,128)(2,1)} %all-gather.18.cloned.1.call-done), kind=kOutput, calls=%fused_computation.38 | convolution fusion | flops 2952790016 | bytes 10747904 | tf_op jit(solution)/shard_map/dot_general | solution.py:64
  362.6 15.8 %all-gather.20.cloned.1.call-done = bf16[2048,1408]{1,0:T(8,128)(2,1)} async-done(((bf16[512,1408]{1,0:T(8,128)(2,1)}), bf16[2048,1408]{1,0:T(8,128)(2,1)}) %all-gather.20.cloned.1.call-update) | async-done | bytes 5767184 | tf_op jit(solution)/shard_map/all_gather | solution.py:61
  378.4 14.0 %fusion.6 = bf16[512,2048]{1,0:T(8,128)(2,1)} fusion(bf16[1408,4096]{1,0:T(8,128)(2,1)} %constant_dynamic-update-slice_fusion, s32[]{:T(128)S(6)} %select_n.18, bf16[512,2048]{1,0:T(8,128)(2,1)} %all-gather.16.cloned.1.call-done, bf16[2048,1408]{1,0:T(8,128)(2,1)} %all-gather.20.cloned.1.call-done, f32[512,1408]{1,0:T(8,128)} %fusion.22), kind=kOutput, calls=%fused_computation.9 | convolution fusion | flops 5910953984 | bytes 18612228 | tf_op jit(solution)/shard_map/dot_general | solution.py:74
  392.4 9.9 %reduce-scatter.5.cloned.1.call-done = bf16[256,2048]{1,0:T(8,128)(2,1)} async-done(((bf16[512,2048]{1,0:T(8,128)(2,1)}), bf16[256,2048]{1,0:T(8,128)(2,1)}) %reduce-scatter.5.cloned.1.call-update) | async-done | bytes 1048592 | tf_op jit(solution)/shard_map/reduce_scatter | solution.py:73
  402.4 2.7 add_convert_fusion
  (46 shorter events, 12.7 us)
Async XLA Ops:
  6.5 2.8 copy-start
  6.5 3.3 copy-start.6
  6.5 40.6 %copy-start.7 = (f32[2048]{0:T(1024)S(1)}, f32[2048]{0:T(1024)}, u32[]{:S(2)}) copy-start(f32[2048]{0:T(1024)} %param.12) | copy-start | bytes 24580
  6.5 40.6 %all-gather.10.cloned.1.call-start = ((), (), s32[]{:S(2)}) async-start(), calls=%async_computation.3 | async-start | bytes 2621440 | tf_op jit(solution)/shard_map/all_gather | solution.py:41
  7.3 76.9 %all-gather.12.cloned.1.call-start = ((), (), s32[]{:S(2)}) async-start(), calls=%async_computation.4 | async-start | bytes 2621440 | tf_op jit(solution)/shard_map/all_gather | solution.py:42
  8.0 113.1 %all-gather.14.cloned.1.call-start = ((), (), s32[]{:S(2)}) async-start(), calls=%async_computation.5 | async-start | bytes 2621440 | tf_op jit(solution)/shard_map/all_gather | solution.py:48
  8.7 149.2 %all-gather.8.cloned.1.call-start = ((), (), s32[]{:S(2)}) async-start(), calls=%async_computation.2 | async-start | bytes 2621440 | tf_op jit(solution)/shard_map/all_gather | solution.py:40
  9.3 164.6 %reduce-scatter.3.cloned.1.call-start = ((), (), s32[]{:S(2)}) async-start(), calls=%async_computation.6 | async-start | bytes 3145728 | tf_op jit(solution)/shard_map/reduce_scatter | solution.py:50
  164.0 11.6 %copy-start.5 = (f32[2048]{0:T(1024)S(1)}, f32[2048]{0:T(1024)}, u32[]{:S(2)}) copy-start(f32[2048]{0:T(1024)} %param.18) | copy-start | bytes 24580
  164.0 190.2 %all-gather.18.cloned.1.call-start = ((), (), s32[]{:S(2)}) async-start(), calls=%async_computation.8 | async-start | bytes 7208960 | tf_op jit(solution)/shard_map/all_gather | solution.py:60
  164.6 189.7 %all-gather.16.cloned.1.call-start = ((), (), s32[]{:S(2)}) async-start(), calls=%async_computation.7 | async-start | bytes 3145728 | tf_op jit(solution)/shard_map/all_gather | solution.py:63
  173.9 1.8 copy-start.1
  177.1 201.3 %all-gather.20.cloned.1.call-start = ((), (), s32[]{:S(2)}) async-start(), calls=%async_computation.9 | async-start | bytes 7208960 | tf_op jit(solution)/shard_map/all_gather | solution.py:61
  177.9 224.5 %reduce-scatter.5.cloned.1.call-start = ((), (), s32[]{:S(2)}) async-start(), calls=%async_computation.10 | async-start | bytes 3145728 | tf_op jit(solution)/shard_map/reduce_scatter | solution.py:73
  177.9 52.0 %collective-permute-start = (bf16[1408,512]{1,0:T(8,128)(2,1)}, bf16[1408,512]{1,0:T(8,128)(2,1)S(1)}, u32[]{:S(2)}, u32[]{:S(2)}) collective-permute-start(bf16[1408,512]{1,0:T(8,128)(2,1)} %param.21), channel_id=1, source_target_pairs={{0,2},{2,4},{4,6},{6,0},{1,3},{3,5},{5,7},{7,1},{8,10},{10,12},{12... | collective-permute-start | bytes 4325384 | tf_op jit(solution)/shard_map/ppermute | solution.py:69
  230.0 1.2 copy-start.3
  231.1 59.1 %collective-permute-start.1 = (bf16[1408,512]{1,0:T(8,128)(2,1)S(1)}, bf16[1408,512]{1,0:T(8,128)(2,1)}, u32[]{:S(2)}, u32[]{:S(2)}) collective-permute-start(bf16[1408,512]{1,0:T(8,128)(2,1)S(1)} %collective-permute-done), channel_id=1, source_target_pairs={{0,2},{2,4},{4,6},{6,0},{1,3},{3,5},{5,7},{7,1},{8,10},{10,12},{12... | collective-permute-start | bytes 4325384 | tf_op jit(solution)/shard_map/ppermute | solution.py:69
  290.3 47.6 %collective-permute-start.2 = (bf16[1408,512]{1,0:T(8,128)(2,1)}, bf16[1408,512]{1,0:T(8,128)(2,1)}, u32[]{:S(2)}, u32[]{:S(2)}) collective-permute-start(bf16[1408,512]{1,0:T(8,128)(2,1)} %collective-permute-done.1), channel_id=1, source_target_pairs={{0,2},{2,4},{4,6},{6,0},{1,3},{3,5},{5,7},{7,1},{8,10},{10,12},{12... | collective-permute-start | bytes 4325384 | tf_op jit(solution)/shard_map/ppermute | solution.py:69
  340.5 2.8 copy-start.4
  343.2 1.9 copy-start.2
Sparse Core Ops, SparseCore 0:
  9.2 37.8 all-gather.9
  49.0 35.1 all-gather.11
  86.0 35.0 all-gather.13
  122.8 35.1 all-gather.7
  164.1 9.7 reduce-scatter.2
  175.6 109.3 all-gather.17
  286.6 10.6 all-gather.15
  299.1 79.2 all-gather.19
  392.6 9.7 reduce-scatter.4
